TPU v7x, 512 devices: a 4x2x32 block of a 4x8x32 slice. The times are simulated.
512 devices in a mesh: grp: 2 (over y), sp: 32 (over z), dp: 8 (over x, core).
Axes of the slice: x: 4, y: 2, z: 32, core: 2. Of those that a mesh axis runs over, the one named last changes fastest.
The devices are a block of a 4x8x32 slice.
Arguments:
- tokens: bfloat16 [16, 12288, 2048], P(('grp', 'dp'), 'sp'), parts along dimension 0, may hold values from -6 to 6
- w_value: bfloat16 [2048, 1024], P('dp', 'sp'), may hold values from -0.125 to 0.125
- w_gate: bfloat16 [2048, 1024], P('dp', 'sp'), may hold values from -0.125 to 0.125
- conv_weight: bfloat16 [31, 1024], replicated, may hold values from -20 to 20
- norm_gain: float32 [1024], replicated, may hold values from 0.1 to 1.9
- norm_bias: float32 [1024], replicated, may hold values from -3 to 3
- w_out: bfloat16 [1024, 2048], P('sp', 'dp'), may hold values from -0.1875 to 0.1875
Outputs:
- mixed: bfloat16 [16, 12288, 2048], P(('grp', 'dp'), 'sp'), parts along dimension 0
There are 2 independent parts, one for each index of `grp`. A program takes and returns all parts, laid end to end along the dimension named above; an argument that names none is the same for every part. Nothing has to cross between parts.
All inputs are finite; a program needn't handle non-finite values.
Results may differ from a plain program's by a relative error of at most 0.012.
Values may be sent and summed in bfloat16 or wider, within the bound.
No kernel may reach another device: no remote copies, remote signals or barrier semaphores. Data moves between devices by JAX's collectives and lax.ppermute only.
A program may use at most 64 MiB of HBM per device.

v0:
```python
import jax
import jax.numpy as jnp
from jax import lax
from jax.sharding import PartitionSpec as P

EPS = 1e-05


def rows_first(arrays, axis, dims):
    turned = [jnp.moveaxis(a, dim, 0) for a, dim in zip(arrays, dims)]
    both = jnp.concatenate([t.reshape(len(t), -1) for t in turned], axis=1)
    out, at, finished = (lax.all_gather(both, axis, axis=0, tiled=True), 0, [])
    for t, dim in zip(turned, dims):
        share = out[:, at : at + t[0].size].reshape(-1, *t.shape[1:])
        finished.append(jnp.moveaxis(share, 0, dim))
        at += t[0].size
    return tuple(finished)


def passed_along(array, axis, by):
    peers = lax.axis_size(axis)
    pairs = [(i, i + by) for i in range(peers) if 0 <= i + by < peers]
    return lax.ppermute(array, axis, pairs)


def per_device(tokens, w_value, w_gate, conv_weight, norm_gain, norm_bias, w_out):
    pieces = rows_first((w_value, w_gate, w_out), "dp", (0, 0, 1))
    full_value, full_gate, full_out = rows_first((pieces[0], pieces[1], pieces[2]), "sp", (1, 1, 0))
    rows = tokens[0]
    kernel_width = conv_weight.shape[0]
    channels = norm_gain.shape[0]
    value = jnp.dot(rows, full_value, preferred_element_type=jnp.float32)
    gate = jnp.dot(rows, full_gate, preferred_element_type=jnp.float32)
    glu = (value * jax.nn.sigmoid(gate)).astype(jnp.bfloat16)
    earlier = passed_along(glu[rows.shape[0] - (kernel_width - 1) :], "sp", 1)
    extended = jnp.concatenate([earlier, glu], axis=0)
    kernel = conv_weight[::-1][:, None, :]
    conv = lax.conv_general_dilated(
        extended[None],
        kernel,
        (1,),
        [(0, 0)],
        dimension_numbers=("NWC", "WIO", "NWC"),
        feature_group_count=channels,
        preferred_element_type=jnp.float32,
    )[0].astype(jnp.bfloat16)
    conv_f = conv.astype(jnp.float32)
    mean = jnp.mean(conv_f, axis=1, keepdims=True)
    meansq = jnp.mean(conv_f * conv_f, axis=1, keepdims=True)
    scaled = (conv_f - mean) * lax.rsqrt(meansq - mean * mean + EPS) * norm_gain + norm_bias
    normed = jax.nn.silu(scaled).astype(jnp.bfloat16)
    mixed = jnp.dot(normed, full_out, preferred_element_type=jnp.float32)
    return mixed.astype(jnp.bfloat16)[None]


def solution(mesh):
    placed = (
        P(("grp", "dp"), "sp", None),
        P("dp", "sp"),
        P("dp", "sp"),
        P(),
        P(),
        P(),
        P("sp", "dp"),
    )
    return jax.shard_map(
        per_device,
        mesh=mesh,
        in_specs=placed,
        out_specs=P(("grp", "dp"), "sp", None),
        check_vma=False,
    )
```

profile of v0, /device:TPU:34, one launch (start us, length us, event | category | flops | bytes accessed | tf_op | source)
XLA Modules:
  0.0 246.4 jit_solution(5164028319720590578)
XLA Ops:
  6.5 0.0 copy-start
  6.6 0.0 all-gather.2.cloned.1.call-start
  6.6 0.9 pad_maximum_fusion.1
  7.4 50.4 %all_gather.6 = bf16[2048,96]{0,1:T(8,128)(2,1)S(1)} all-gather(bf16[256,96]{0,1:T(8,128)(2,1)S(1)} %pad_maximum_fusion.1), channel_id=1, replica_groups=mesh['grp'=2,'sp'=32,'dp'=8] {'dp'}, dimensions={0}, use_global_device_ids=true | all-gather | bytes 442368 | tf_op jit(solution)/shard_map/all_gather | solution.py:12
  57.9 0.8 pad_maximum_fusion
  58.7 0.1 all-gather.2.cloned.1.call-update
  58.7 153.0 %all-gather.2.cloned.1.call-done = bf16[1024,6144]{1,0:T(8,128)(2,1)} async-done(((bf16[32,6144]{1,0:T(8,128)(2,1)}), bf16[1024,6144]{1,0:T(8,128)(2,1)}) %all-gather.2.cloned.1.call-update) | async-done | bytes 12582928 | tf_op jit(solution)/shard_map/all_gather | solution.py:12
  211.7 0.0 copy-done
  211.7 4.0 %fusion.2 = f32[1024,384]{0,1:T(8,128)S(1)} fusion(bf16[1024,6144]{1,0:T(8,128)(2,1)} %all-gather.2.cloned.1.call-done, bf16[1,384,2048]{2,1,0:T(8,128)(2,1)S(1)} %copy-done), kind=kOutput, calls=%fused_computation.2 | convolution fusion | flops 1610612736 | bytes 7340032 | tf_op jit(solution)/shard_map/dot_general | solution.py:33
  215.7 0.0 copy-start.1
  215.8 4.1 %fusion.30 = bf16[384,1024]{1,0:T(8,128)(2,1)S(1)} fusion(f32[1024,384]{0,1:T(8,128)S(1)} %fusion.2, bf16[1,384,2048]{2,1,0:T(8,128)(2,1)S(1)} %copy-done, bf16[1024,6144]{1,0:T(8,128)(2,1)} %all-gather.2.cloned.1.call-done), kind=kOutput, calls=%fused_computation.28 | convolution fusion | flops 1612578816 | bytes 8126464 | tf_op jit(solution)/shard_map/dot_general | solution.py:32
  219.9 3.0 %collective-permute-start = (bf16[30,1024]{1,0:T(8,128)(2,1)S(1)}, bf16[30,1024]{1,0:T(8,128)(2,1)S(1)}, u32[]{:S(2)}, u32[]{:S(2)}) collective-permute-start(bf16[30,1024]{1,0:T(8,128)(2,1)S(1)} %slice.35), channel_id=1, source_target_pairs={{0,8},{8,16},{16,24},{24,32},{32,40},{40,48},{48,56},{56,64},{64,7... | collective-permute-start | bytes 184328 | tf_op jit(solution)/shard_map/ppermute | solution.py:23
  222.9 0.0 copy-done.1
  222.9 0.3 rev.3
  223.2 1.4 collective-permute-done
  224.6 0.2 maximum_bitcast_fusion
  224.8 0.1 pad
  224.9 0.2 reshape.24
  225.0 0.0 copy-start.4
  225.1 0.5 copy.12
  225.5 0.1 slice.36
  225.7 0.1 copy-done.4
  225.7 3.8 %fusion.37 = f32[8,52,1024]{2,0,1:T(8,128)S(1)} fusion(bf16[1,7,30,1024]{3,1,2,0:T(8,128)(2,1)S(1)} %slice.36, bf16[1,8,52,1024]{3,1,2,0:T(8,128)(2,1)S(1)} %copy.12, pred[8,52]{0,1:T(8,128)(4,1)S(1)} %copy-done.4, bf16[31,1,1024]{2,0,1:T(8,128)(2,1)S(1)} %bitcast.44), kind=kOutput, calls=%fused_computation.29 | convolution fusion | flops 31719424 | bytes 3049888 | tf_op jit(solution)/shard_map/conv_general_dilated | solution.py:38
  229.5 2.3 copy.14
  231.8 1.6 reshape.28
  233.4 0.0 copy-start.2
  233.4 0.0 copy-start.3
  233.4 0.2 fusion.16
  233.6 0.2 slice_reduce_fusion
  233.7 0.3 copy-done.2
  234.0 0.0 copy-done.3
  234.1 5.5 %fusion.10 = bf16[1,384,2048]{2,1,0:T(8,128)(2,1)} fusion(bf16[1024,6144]{1,0:T(8,128)(2,1)} %all-gather.2.cloned.1.call-done, f32[1,416,1024]{2,1,0:T(8,128)S(1)} %reshape.28, f32[1024]{0:T(1024)S(1)} %copy-done.2, f32[1024]{0:T(1024)S(1)} %copy-done.3, f32[384]{0:T(512)S(1)} %get-tuple-element.9, f32[384]{0:T(512)S(1)} %get-tuple-element.8), kind=kOutput, calls=%fused_computation.9 | convolution fusion | flops 1614938112 | bytes 7352320 | tf_op jit(solution)/shard_map/dot_general | solution.py:52
  (3 shorter events, 0.1 us)
Async XLA Ops:
  6.5 205.2 %copy-start = (bf16[1,384,2048]{2,1,0:T(8,128)(2,1)S(1)}, bf16[1,384,2048]{2,1,0:T(8,128)(2,1)}, u32[]{:S(2)}) copy-start(bf16[1,384,2048]{2,1,0:T(8,128)(2,1)} %param.7) | copy-start | bytes 4718596
  6.6 205.2 %all-gather.2.cloned.1.call-start = ((), (), s32[]{:S(2)}) async-start(), calls=%async_computation | async-start | bytes 12976128 | tf_op jit(solution)/shard_map/all_gather | solution.py:12
  215.7 7.2 %copy-start.1 = (bf16[31,1024]{1,0:T(8,128)(2,1)S(1)}, bf16[31,1024]{1,0:T(8,128)(2,1)}, u32[]{:S(2)}) copy-start(bf16[31,1024]{1,0:T(8,128)(2,1)} %param.10) | copy-start | bytes 190468
  219.9 4.7 %collective-permute-start = (bf16[30,1024]{1,0:T(8,128)(2,1)S(1)}, bf16[30,1024]{1,0:T(8,128)(2,1)S(1)}, u32[]{:S(2)}, u32[]{:S(2)}) collective-permute-start(bf16[30,1024]{1,0:T(8,128)(2,1)S(1)} %slice.35), channel_id=1, source_target_pairs={{0,8},{8,16},{16,24},{24,32},{32,40},{40,48},{48,56},{56,64},{64,7... | collective-permute-start | bytes 184328 | tf_op jit(solution)/shard_map/ppermute | solution.py:23
  225.0 0.7 copy-start.4
  233.4 0.7 copy-start.2
  233.4 0.7 copy-start.3
Sparse Core Ops, SparseCore 0:
  58.9 152.8 all-gather.1
where the time goes:
time: 247 us; the launch traced here: 246 us
  waiting for transfers between devices  154 us (62%)
  blocking collectives  50.4 us (20%)
  matrix products  17.4 us (7%)
  between operations  13.6 us (6%)
  local copies, waits for them, and re-layouts  5.38 us (2%)
  starting transfers between devices  2.97 us (1%)
    all_gather x1, waiting for transfers between devices, rows_first(): out, at, finished = (lax.all_gather(both, axis, axis=0, tiled=True), 0, [])  153 us
    all_gather x1, blocking collectives, rows_first(): out, at, finished = (lax.all_gather(both, axis, axis=0, tiled=True), 0, [])  50.4 us
    dot_general x1, matrix products, per_device(): mixed = jnp.dot(normed, full_out, preferred_element_type=jnp.float32)  5.51 us
  transfers between devices with their start and end apart: 2, of which 2 were waited for; matrix products, arithmetic and copies ran while one was open for 0% of the time, Pallas kernels for 0%

commit v1 on v0

--- a/solution.py
+++ b/solution.py
@@ -6,10 +6,15 @@
 EPS = 1e-05
 
 
+def gather_over(x, name, d):
+    sent = jnp.stack([x] * lax.axis_size(name))
+    return jnp.concatenate(lax.all_to_all(sent, name, 0, 0), axis=d)
+
+
 def rows_first(arrays, axis, dims):
     turned = [jnp.moveaxis(a, dim, 0) for a, dim in zip(arrays, dims)]
     both = jnp.concatenate([t.reshape(len(t), -1) for t in turned], axis=1)
-    out, at, finished = (lax.all_gather(both, axis, axis=0, tiled=True), 0, [])
+    out, at, finished = (gather_over(both, axis, 0), 0, [])
     for t, dim in zip(turned, dims):
         share = out[:, at : at + t[0].size].reshape(-1, *t.shape[1:])
         finished.append(jnp.moveaxis(share, 0, dim))

time: 247 us -> 1190 us (4.82)
  the two profiles are of different devices: /device:TPU:34 before, /device:TPU:40 now
where the time goes in v1:
time: 1190 us
  blocking collectives  1150 us (97%)
  local copies, waits for them, and re-layouts  14.3 us (1%)
  matrix products  13 us (1%)
    all_to_all x2, blocking collectives, gather_over(): return jnp.concatenate(lax.all_to_all(sent, name, 0, 0), axis=d)  1150 us
  transfers between devices with their start and end apart: 1, of which 1 were waited for; matrix products, arithmetic and copies ran while one was open for 0% of the time, Pallas kernels for 0%

profile of v1, /device:TPU:40, one launch (start us, length us, event | category | flops | bytes accessed | tf_op | source)
XLA Modules:
  0.0 1187.2 jit_solution(14321873557777999477)
XLA Ops:
  0.0 0.0 copy-start
  0.0 0.9 pad_maximum_fusion.1
  0.9 13.3 %all_to_all.10 = bf16[8,256,96]{1,2,0:T(8,128)(2,1)S(1)} all-to-all(bf16[8,256,96]{1,2,0:T(8,128)(2,1)S(1)} %stack.4), channel_id=1, replica_groups=mesh['grp'=2,'sp'=32,'dp'=8] {'dp'}, dimensions={0} | all-to-all | bytes 786432 | tf_op jit(solution)/shard_map/all_to_all | solution.py:11
  14.3 6.1 stack.5
  20.4 1138.5 %all_to_all.11 = bf16[32,32,6144]{2,1,0:T(8,128)(2,1)S(1)} all-to-all(bf16[32,32,6144]{2,1,0:T(8,128)(2,1)} %stack.5), channel_id=1, replica_groups=mesh['grp'=2,'sp'=32,'dp'=8] {'sp'}, dimensions={0} | all-to-all | bytes 25165824 | tf_op jit(solution)/shard_map/all_to_all | solution.py:11
  1159.0 0.0 copy-start.1
  1159.0 0.0 copy-done
  1159.0 1.8 fusion.2
  1160.8 2.7 copy-done.1
  1163.5 0.0 copy-start.2
  1163.5 1.9 fusion.30
  1165.5 5.0 collective-permute-start
  1170.5 0.0 copy-done.2
  1170.5 0.3 rev.3
  1170.8 1.4 collective-permute-done
  1172.2 0.2 maximum_bitcast_fusion
  1172.4 0.1 pad
  1172.5 0.2 reshape.36
  1172.6 0.0 copy-start.5
  1172.7 0.5 copy.25
  1173.1 0.1 slice.36
  1173.3 0.1 copy-done.5
  1173.3 3.8 fusion.37
  1177.1 2.3 copy.27
  1179.4 1.6 reshape.40
  1181.0 0.0 copy-start.3
  1181.0 0.0 copy-start.4
  1181.0 0.2 fusion.16
  1181.2 0.2 slice_reduce_fusion
  1181.3 0.3 copy-done.3
  1181.7 0.0 copy-done.4
  1181.7 5.5 fusion.10
  (6 shorter events, 0.1 us)
Async XLA Ops:
  0.0 1159.0 %copy-start = (bf16[1,384,2048]{2,1,0:T(8,128)(2,1)S(1)}, bf16[1,384,2048]{2,1,0:T(8,128)(2,1)}, u32[]{:S(2)}) copy-start(bf16[1,384,2048]{2,1,0:T(8,128)(2,1)} %param.7) | copy-start | bytes 4718596
  1159.0 4.5 copy-start.1
  1163.5 7.0 copy-start.2
  1165.5 6.7 collective-permute-start
  1172.6 0.7 copy-start.5
  1181.0 0.7 copy-start.3
  1181.0 0.7 copy-start.4
